TPU v7x, 32 devices: a whole 2x2x4 slice. The times are simulated.
32 devices in a mesh: rep: 4 (over y, x), fs: 2 (over core), tp: 4 (over z).
Axes of the slice: x: 2, y: 2, z: 4, core: 2. Of those that a mesh axis runs over, the one named last changes fastest.
Arguments:
- layer_input: bfloat16 [10240, 2048], P(('rep', 'fs'), 'tp'), may hold values from -6 to 6
- cotangent: bfloat16 [10240, 2048], P(('rep', 'fs'), 'tp'), may hold values from -8 to 8
- gate_pre: bfloat16 [10240, 3072], P('rep', 'fs'), may hold values from -8 to 8
- up_pre: bfloat16 [10240, 3072], P('rep', 'fs'), may hold values from -6 to 6
- gate_weight: bfloat16 [2048, 3072], P('tp', 'fs'), may hold values from -0.125 to 0.125
- up_weight: bfloat16 [2048, 3072], P('tp', 'fs'), may hold values from -0.125 to 0.125
- down_weight: bfloat16 [3072, 2048], P('fs', 'tp'), may hold values from -0.109375 to 0.109375
Outputs:
- input_grad: bfloat16 [10240, 2048], P(('rep', 'fs'), 'tp')
- gate_grad: float32 [2048, 3072], P('tp', 'fs')
- up_grad: float32 [2048, 3072], P('tp', 'fs')
- down_grad: float32 [3072, 2048], P('fs', 'tp')
- gate_rows_sq: float32 [2048], P('tp')
- up_rows_sq: float32 [2048], P('tp')
- down_rows_sq: float32 [3072], P('fs')
All inputs are finite; a program needn't handle non-finite values.
Results may differ from a plain program's by a relative error of at most 0.019.
Values may be sent and summed in bfloat16 or wider, within the bound.
No kernel may reach another device: no remote copies, remote signals or barrier semaphores. Data moves between devices by JAX's collectives and lax.ppermute only.
A program may use at most 128 MiB of HBM per device.

v0:
```python
import math
import jax
import jax.numpy as jnp
from jax import lax
from jax.sharding import PartitionSpec as P


def contract_rows(left_side, right_side):
    return lax.dot_general(
        left_side, right_side, (((0,), (0,)), ((), ())), preferred_element_type=jnp.float32
    )


def contract_cols(left_side, right_side):
    return lax.dot_general(
        left_side, right_side, (((1,), (1,)), ((), ())), preferred_element_type=jnp.float32
    )


def row_squares(gate_grad, up_grad, down_grad):
    gate_sq = jnp.sum(gate_grad * gate_grad, axis=1)
    up_sq = jnp.sum(up_grad * up_grad, axis=1)
    down_sq = jnp.sum(down_grad * down_grad, axis=1)
    gate_sq, up_sq = lax.psum((gate_sq, up_sq), "fs")
    down_sq = lax.psum(down_sq, "tp")
    return (gate_sq, up_sq, down_sq)


def on_device(layer_input, cotangent, gate_pre, up_pre, gate_weight, up_weight, down_weight):
    group_input, group_cotangent = (
        lax.all_gather(layer_input, "fs", axis=0, tiled=True),
        lax.all_gather(cotangent, "fs", axis=0, tiled=True),
    )
    hidden_grad = lax.psum(
        contract_cols(group_cotangent, down_weight).astype(jnp.bfloat16), "tp"
    ).astype(jnp.float32)
    gate_value = gate_pre.astype(jnp.float32)
    up_value = up_pre.astype(jnp.float32)
    sigmoid_gate = jax.nn.sigmoid(gate_value)
    activated = gate_value * sigmoid_gate
    hidden = (activated * up_value).astype(jnp.bfloat16)
    gate_delta = (
        hidden_grad * up_value * sigmoid_gate * (1.0 + gate_value * (1.0 - sigmoid_gate))
    ).astype(jnp.bfloat16)
    up_delta = (hidden_grad * activated).astype(jnp.bfloat16)
    input_grad = lax.psum_scatter(
        (contract_cols(gate_delta, gate_weight) + contract_cols(up_delta, up_weight)).astype(
            jnp.bfloat16
        ),
        "fs",
        scatter_dimension=0,
        tiled=True,
    )
    grad_scale = 1.0 / math.sqrt(group_input.shape[0] * lax.axis_size("rep"))
    gate_grad = contract_rows(group_input, gate_delta) * grad_scale
    up_grad = contract_rows(group_input, up_delta) * grad_scale
    down_grad = contract_rows(hidden, group_cotangent) * grad_scale
    gate_grad, up_grad, down_grad = (
        lax.psum(gate_grad.astype(jnp.bfloat16), "rep").astype(jnp.float32),
        lax.psum(up_grad.astype(jnp.bfloat16), "rep").astype(jnp.float32),
        lax.psum(down_grad.astype(jnp.bfloat16), "rep").astype(jnp.float32),
    )
    gate_sq, up_sq, down_sq = row_squares(gate_grad, up_grad, down_grad)
    return (input_grad, gate_grad, up_grad, down_grad, gate_sq, up_sq, down_sq)


def solution(mesh):
    return jax.shard_map(
        on_device,
        mesh=mesh,
        in_specs=(
            P(("rep", "fs"), "tp"),
            P(("rep", "fs"), "tp"),
            P("rep", "fs"),
            P("rep", "fs"),
            P("tp", "fs"),
            P("tp", "fs"),
            P("fs", "tp"),
        ),
        out_specs=(
            P(("rep", "fs"), "tp"),
            P("tp", "fs"),
            P("tp", "fs"),
            P("fs", "tp"),
            P("tp"),
            P("tp"),
            P("fs"),
        ),
        check_vma=False,
    )
```

profile of v0, /device:TPU:0, one launch (start us, length us, event | category | flops | bytes accessed | tf_op | source)
XLA Modules:
  0.0 484.3 jit_solution(10853355649280223357)
XLA Ops:
  7.2 0.0 copy-start
  7.2 0.0 all-gather.3.cloned.1.call-start
  7.2 0.7 all-gather.3.cloned.1.call-update
  7.9 0.0 all-reduce.5.cloned.1.call-start
  8.0 15.7 %all-gather.3.cloned.1.call-done = bf16[2560,512]{1,0:T(8,128)(2,1)} async-done(((bf16[1280,512]{1,0:T(8,128)(2,1)}), bf16[2560,512]{1,0:T(8,128)(2,1)}) %all-gather.3.cloned.1.call-update) | async-done | bytes 2621456 | tf_op jit(solution)/shard_map/all_gather | solution.py:32
  23.6 0.0 copy-done
  23.6 8.2 %convolution_convert_fusion = bf16[2560,1536]{1,0:T(8,128)(2,1)} fusion(bf16[2560,512]{1,0:T(8,128)(2,1)} %all-gather.3.cloned.1.call-done, bf16[1536,512]{1,0:T(8,128)(2,1)S(1)} %copy-done), kind=kOutput, calls=%fused_computation.15 | convolution fusion | flops 4030464000 | bytes 12058624 | tf_op jit(solution)/shard_map/dot_general | solution.py:15
  31.9 0.0 all-reduce.5.cloned.1.call-update
  31.9 0.0 all-gather.5.cloned.1.call-start
  32.0 0.7 all-gather.5.cloned.1.call-update
  32.6 0.0 all-reduce.7.cloned.1.call-start
  32.7 10.0 %fusion.14 = bf16[1536,512]{1,0:T(8,128)(2,1)} fusion(bf16[2560,512]{1,0:T(8,128)(2,1)} %all-gather.3.cloned.1.call-done, bf16[2560,1536]{1,0:T(8,128)(2,1)} %param.10, bf16[2560,1536]{1,0:T(8,128)(2,1)} %param.9), kind=kOutput, calls=%fused_computation.24 | convolution fusion | flops 4059561984 | bytes 19922944 | tf_op jit(solution)/shard_map/dot_general | solution.py:9
  42.7 264.3 %all-reduce.5.cloned.1.call-done = bf16[2560,1536]{1,0:T(8,128)(2,1)} async-done(((bf16[2560,1536]{1,0:T(8,128)(2,1)}), bf16[2560,1536]{1,0:T(8,128)(2,1)}) %all-reduce.5.cloned.1.call-update) | async-done | bytes 7864336 | tf_op jit(solution)/shard_map/psum | solution.py:34
  307.0 17.0 %fusion = (bf16[2560,1536]{1,0:T(8,128)(2,1)}, bf16[2560,1536]{1,0:T(8,128)(2,1)}) fusion(bf16[2560,1536]{1,0:T(8,128)(2,1)} %all-reduce.5.cloned.1.call-done, bf16[2560,1536]{1,0:T(8,128)(2,1)} %param.9, bf16[2560,1536]{1,0:T(8,128)(2,1)} %param.10), kind=kLoop, calls=%fused_computation.6 | loop fusion | flops 62914560 | bytes 39321600 | tf_op jit(solution)/shard_map/convert_element_type | solution.py:45
  324.1 9.6 %fusion.20 = bf16[512,1536]{0,1:T(8,128)(2,1)} fusion(bf16[2560,1536]{1,0:T(8,128)(2,1)} %get-tuple-element.22, bf16[2560,512]{1,0:T(8,128)(2,1)} %all-gather.5.cloned.1.call-done), kind=kOutput, calls=%fused_computation.28 | convolution fusion | flops 4028104704 | bytes 12058624 | tf_op jit(solution)/shard_map/dot_general | solution.py:9
  333.6 0.0 copy-done.2
  333.6 0.0 copy-done.4
  333.6 5.4 %fusion.19 = bf16[512,1536]{0,1:T(8,128)(2,1)} fusion(bf16[2560,1536]{1,0:T(8,128)(2,1)S(1)} %copy-done.2, bf16[2560,512]{1,0:T(8,128)(2,1)S(1)} %copy-done.4), kind=kOutput, calls=%fused_computation.27 | convolution fusion | flops 4028104704 | bytes 12058624 | tf_op jit(solution)/shard_map/dot_general | solution.py:9
  339.0 0.0 all-reduce.7.cloned.1.call-update
  339.0 0.0 copy-start.6
  339.0 0.2 reduce-scatter.2.cloned.1.call-start
  339.3 0.0 copy-done.5
  339.3 6.9 %fusion.22 = f32[2560,512]{1,0:T(8,128)S(1)} fusion(bf16[2560,1536]{1,0:T(8,128)(2,1)} %get-tuple-element.22, bf16[512,1536]{1,0:T(8,128)(2,1)S(1)} %copy-done.5), kind=kOutput, calls=%fused_computation.30 | convolution fusion | flops 4026531840 | bytes 14680064 | tf_op jit(solution)/shard_map/dot_general | solution.py:15
  346.2 9.2 %add_convert_fusion = bf16[2560,512]{1,0:T(8,128)(2,1)} fusion(f32[2560,512]{1,0:T(8,128)S(1)} %fusion.22, bf16[2560,1536]{1,0:T(8,128)(2,1)} %get-tuple-element.21, bf16[512,1536]{1,0:T(8,128)(2,1)S(1)} %copy-done.6), kind=kOutput, calls=%fused_computation.17 | convolution fusion | flops 4029153280 | bytes 17301504 | tf_op jit(solution)/shard_map/dot_general | solution.py:15
  355.4 0.0 reduce-scatter.2.cloned.1.call-update
  355.4 94.9 %all-reduce.7.cloned.1.call-done = (bf16[512,1536]{0,1:T(8,128)(2,1)}, bf16[512,1536]{0,1:T(8,128)(2,1)}, bf16[1536,512]{1,0:T(8,128)(2,1)}) async-done(((bf16[512,1536]{0,1:T(8,128)(2,1)}, bf16[512,1536]{0,1:T(8,128)(2,1)}, bf16[1536,512]{1,0:T(8,128)(2,1)}), (bf16[512,1536]{0,1:T(8,128)(2,1)}, bf16[512,1536]{0,1:T(8,128)(2,1)}, bf16[1536,512]{1,0:T(8,128)(2,1)})) %all-reduce.7.cloned.1.call-update) | async-done | bytes 4718608 | tf_op jit(solution)/shard_map/psum | solution.py:59
  450.4 3.2 copy.14
  453.5 3.2 copy.15
  456.7 2.1 multiply_reduce_fusion.1
  458.8 3.0 all-reduce
  461.8 3.5 multiply_reduce_fusion
  465.3 12.4 %psum.55 = f32[1536]{0:T(1024)} all-reduce(f32[1536]{0:T(1024)S(1)} %get-tuple-element.19), channel_id=1, replica_groups=mesh['rep'=4,'fs'=2,'tp'=4] {'tp'}, use_global_device_ids=true, to_apply=%region_10.0 | all-reduce | flops 1536 | bytes 12288 | tf_op jit(solution)/shard_map/psum | solution.py:25
  (10 shorter events, 0.0 us)
Async XLA Ops:
  7.2 16.5 %copy-start = (bf16[1536,512]{1,0:T(8,128)(2,1)S(1)}, bf16[1536,512]{1,0:T(8,128)(2,1)}, u32[]{:S(2)}) copy-start(bf16[1536,512]{1,0:T(8,128)(2,1)} %param.13) | copy-start | bytes 4718596
  7.2 16.5 %all-gather.3.cloned.1.call-start = ((), (), s32[]{:S(2)}) async-start(), calls=%async_computation.1 | async-start | bytes 3932160 | tf_op jit(solution)/shard_map/all_gather | solution.py:32
  7.9 299.1 %all-reduce.5.cloned.1.call-start = ((), (), s32[]{:S(2)}) async-start(), calls=%async_computation.2 | async-start | bytes 15728640 | tf_op jit(solution)/shard_map/psum | solution.py:34
  31.9 292.1 %all-gather.5.cloned.1.call-start = ((), (), s32[]{:S(2)}) async-start(), calls=%async_computation.4 | async-start | bytes 3932160 | tf_op jit(solution)/shard_map/all_gather | solution.py:31
  32.6 417.7 %all-reduce.7.cloned.1.call-start = ((), (), s32[]{:S(2)}) async-start(), calls=%async_computation.5 | async-start | bytes 9437184 | tf_op jit(solution)/shard_map/psum | solution.py:59
  324.1 9.6 %copy-start.2 = (bf16[2560,1536]{1,0:T(8,128)(2,1)S(1)}, bf16[2560,1536]{1,0:T(8,128)(2,1)}, u32[]{:S(2)}) copy-start(bf16[2560,1536]{1,0:T(8,128)(2,1)} %get-tuple-element.21) | copy-start | bytes 23592964
  324.1 9.6 %copy-start.4 = (bf16[2560,512]{1,0:T(8,128)(2,1)S(1)}, bf16[2560,512]{1,0:T(8,128)(2,1)}, u32[]{:S(2)}) copy-start(bf16[2560,512]{1,0:T(8,128)(2,1)} %all-gather.5.cloned.1.call-done) | copy-start | bytes 7864324
  333.6 5.7 %copy-start.5 = (bf16[512,1536]{1,0:T(8,128)(2,1)S(1)}, bf16[512,1536]{1,0:T(8,128)(2,1)}, u32[]{:S(2)}) copy-start(bf16[512,1536]{1,0:T(8,128)(2,1)} %param.11) | copy-start | bytes 4718596
  339.0 7.1 %copy-start.6 = (bf16[512,1536]{1,0:T(8,128)(2,1)S(1)}, bf16[512,1536]{1,0:T(8,128)(2,1)}, u32[]{:S(2)}) copy-start(bf16[512,1536]{1,0:T(8,128)(2,1)} %param.12) | copy-start | bytes 4718596
  339.0 138.7 %reduce-scatter.2.cloned.1.call-start = ((), (), s32[]{:S(2)}) async-start(), calls=%async_computation.3 | async-start | bytes 3932160 | tf_op jit(solution)/shard_map/reduce_scatter | solution.py:46
  450.3 6.4 %copy-start.3 = (bf16[512,1536]{0,1:T(8,128)(2,1)S(1)}, bf16[512,1536]{0,1:T(8,128)(2,1)}, u32[]{:S(2)}) copy-start(bf16[512,1536]{0,1:T(8,128)(2,1)} %get-tuple-element.16) | copy-start | bytes 4718596
  453.5 24.2 %copy-start.1 = (bf16[1536,512]{1,0:T(8,128)(2,1)S(1)}, bf16[1536,512]{1,0:T(8,128)(2,1)}, u32[]{:S(2)}) copy-start(bf16[1536,512]{1,0:T(8,128)(2,1)} %param.13) | copy-start | bytes 4718596
Sparse Core Ops, SparseCore 0:
  9.5 14.0 all-gather.2
  32.0 274.9 all-reduce.4
  308.6 10.1 all-gather.4
  339.2 111.1 all-reduce.6
  453.0 10.4 reduce-scatter.1
where the time goes:
time: 485 us; the launch traced here: 484 us
  waiting for transfers between devices  376 us (78%)
  matrix products  49.3 us (10%)
  other arithmetic  22.6 us (5%)
  blocking collectives  15.4 us (3%)
  between operations  13.8 us (3%)
  local copies, waits for them, and re-layouts  6.41 us (1%)
    psum x1, waiting for transfers between devices, on_device(): lax.psum(contract_cols(group_cotangent, down_weight).astype(jnp.bfloat16)...  264 us
    psum x1, waiting for transfers between devices, on_device(): lax.psum(gate_grad.astype(jnp.bfloat16), 'rep').astype(jnp.float32)  94.9 us
    dot_general x3, matrix products, contract_rows(): lax.dot_general(left_side, right_side, (((0,), (0,)), ((), ())), preferre...  25 us
    dot_general x3, matrix products, contract_cols(): lax.dot_general(left_side, right_side, (((1,), (1,)), ((), ())), preferre...  24.3 us
    convert_element_type x1, other arithmetic, on_device(): up_delta = (hidden_grad * activated).astype(jnp.bfloat16)  17 us
    all_gather x1, waiting for transfers between devices, on_device(): lax.all_gather(cotangent, 'fs', axis=0, tiled=True)  15.7 us
    psum x1, blocking collectives, row_squares(): down_sq = lax.psum(down_sq, 'tp')  12.4 us
  transfers between devices with their start and end apart: 5, of which 3 were waited for; matrix products, arithmetic and copies ran while one was open for 11% of the time, Pallas kernels for 0%

commit v1 on v0

--- a/solution.py
+++ b/solution.py
@@ -3,6 +3,7 @@
 import jax.numpy as jnp
 from jax import lax
 from jax.sharding import PartitionSpec as P
+from jax.lax import all_gather
 
 
 def contract_rows(left_side, right_side):
@@ -55,8 +56,13 @@
     gate_grad = contract_rows(group_input, gate_delta) * grad_scale
     up_grad = contract_rows(group_input, up_delta) * grad_scale
     down_grad = contract_rows(hidden, group_cotangent) * grad_scale
+
+    def row_serve(inputs):
+        long_array = jnp.sum(all_gather(inputs, "rep"), axis=0)
+        return long_array
+
     gate_grad, up_grad, down_grad = (
-        lax.psum(gate_grad.astype(jnp.bfloat16), "rep").astype(jnp.float32),
+        row_serve(gate_grad.astype(jnp.bfloat16)).astype(jnp.float32),
         lax.psum(up_grad.astype(jnp.bfloat16), "rep").astype(jnp.float32),
         lax.psum(down_grad.astype(jnp.bfloat16), "rep").astype(jnp.float32),
     )

time: 485 us -> 526 us (1.085)
  waiting for transfers between devices: 376 us -> 396 us
  local copies, waits for them, and re-layouts: 6.41 us -> 16.6 us
  other arithmetic: 22.6 us -> 30.4 us
    all_gather x0 -> x1, waiting for transfers between devices: none -> 54.1 us  [row_serve(): long_array = jnp.sum(all_gather(inputs, 'rep'), axis=0)]
    psum x1, waiting for transfers between devices: 94.9 us -> 60 us  [on_device(): lax.psum(up_grad.astype(jnp.bfloat16), 'rep').astype(jnp.float32)]
    all_gather x0 -> x1, local copies, waits for them, and re-layouts: none -> 11.3 us  [row_serve(): long_array = jnp.sum(all_gather(inputs, 'rep'), axis=0)]
    reduce_sum x0 -> x2, other arithmetic: none -> 11 us  [the longest x1 10.6 us: row_serve(): long_array = jnp.sum(all_gather(inputs, 'rep'), axis=0)]
  transfers between devices with their start and end apart: 5 -> 6, of which waited for: 3 -> 4; matrix products, arithmetic and copies ran while one was open for 11% -> 16% of each run, Pallas kernels for 0% -> 0%
where the time goes in v1:
time: 526 us
  waiting for transfers between devices  396 us (75%)
  matrix products  53.2 us (10%)
  other arithmetic  30.4 us (6%)
  local copies, waits for them, and re-layouts  16.6 us (3%)
  blocking collectives  15.5 us (3%)
  between operations  14.2 us (3%)
    psum x1, waiting for transfers between devices, on_device(): lax.psum(contract_cols(group_cotangent, down_weight).astype(jnp.bfloat16)...  264 us
    psum x1, waiting for transfers between devices, on_device(): lax.psum(up_grad.astype(jnp.bfloat16), 'rep').astype(jnp.float32)  60 us
    all_gather x1, waiting for transfers between devices, row_serve(): long_array = jnp.sum(all_gather(inputs, 'rep'), axis=0)  54.1 us
    dot_general x3, matrix products, contract_rows(): lax.dot_general(left_side, right_side, (((0,), (0,)), ((), ())), preferre...  29 us
    dot_general x3, matrix products, contract_cols(): lax.dot_general(left_side, right_side, (((1,), (1,)), ((), ())), preferre...  24.2 us
    convert_element_type x1, other arithmetic, on_device(): up_delta = (hidden_grad * activated).astype(jnp.bfloat16)  17 us
    all_gather x1, waiting for transfers between devices, on_device(): lax.all_gather(cotangent, 'fs', axis=0, tiled=True)  15.7 us
    psum x1, blocking collectives, row_squares(): down_sq = lax.psum(down_sq, 'tp')  12.5 us
  transfers between devices with their start and end apart: 6, of which 4 were waited for; matrix products, arithmetic and copies ran while one was open for 16% of the time, Pallas kernels for 0%

profile of v1, /device:TPU:0, one launch (start us, length us, event | category | flops | bytes accessed | tf_op | source)
XLA Modules:
  0.0 525.8 jit_solution(13402343585880111398)
XLA Ops:
  7.2 0.0 all-gather.5.cloned.1.call-start
  7.2 0.7 all-gather.5.cloned.1.call-update
  7.9 0.0 all-reduce.5.cloned.1.call-start
  8.0 15.7 %all-gather.5.cloned.1.call-done = bf16[2560,512]{1,0:T(8,128)(2,1)} async-done(((bf16[1280,512]{1,0:T(8,128)(2,1)}), bf16[2560,512]{1,0:T(8,128)(2,1)}) %all-gather.5.cloned.1.call-update) | async-done | bytes 2621456 | tf_op jit(solution)/shard_map/all_gather | solution.py:33
  23.6 8.1 %convolution_convert_fusion = bf16[2560,1536]{1,0:T(8,128)(2,1)} fusion(bf16[2560,512]{1,0:T(8,128)(2,1)} %all-gather.5.cloned.1.call-done, bf16[1536,512]{1,0:T(8,128)(2,1)S(1)} %copy-done), kind=kOutput, calls=%fused_computation.15 | convolution fusion | flops 4030464000 | bytes 12058624 | tf_op jit(solution)/shard_map/dot_general | solution.py:16
  31.8 0.0 all-reduce.5.cloned.1.call-update
  31.8 0.0 all-gather.7.cloned.1.call-start
  31.9 0.7 all-gather.7.cloned.1.call-update
  32.5 0.0 all-reduce.7.cloned.1.call-start
  32.6 10.0 %fusion.14 = bf16[1536,512]{1,0:T(8,128)(2,1)} fusion(bf16[2560,512]{1,0:T(8,128)(2,1)} %all-gather.5.cloned.1.call-done, bf16[2560,1536]{1,0:T(8,128)(2,1)} %param.10, bf16[2560,1536]{1,0:T(8,128)(2,1)} %param.9), kind=kOutput, calls=%fused_computation.24 | convolution fusion | flops 4059561984 | bytes 19922944 | tf_op jit(solution)/shard_map/dot_general | solution.py:10
  42.6 264.3 %all-reduce.5.cloned.1.call-done = bf16[2560,1536]{1,0:T(8,128)(2,1)} async-done(((bf16[2560,1536]{1,0:T(8,128)(2,1)}), bf16[2560,1536]{1,0:T(8,128)(2,1)}) %all-reduce.5.cloned.1.call-update) | async-done | bytes 7864336 | tf_op jit(solution)/shard_map/psum | solution.py:35
  306.9 17.0 %fusion = (bf16[2560,1536]{1,0:T(8,128)(2,1)}, bf16[2560,1536]{1,0:T(8,128)(2,1)}) fusion(bf16[2560,1536]{1,0:T(8,128)(2,1)} %all-reduce.5.cloned.1.call-done, bf16[2560,1536]{1,0:T(8,128)(2,1)} %param.9, bf16[2560,1536]{1,0:T(8,128)(2,1)} %param.10), kind=kLoop, calls=%fused_computation.6 | loop fusion | flops 62914560 | bytes 39321600 | tf_op jit(solution)/shard_map/convert_element_type | solution.py:46
  324.0 9.4 %fusion.19 = bf16[512,1536]{0,1:T(8,128)(2,1)} fusion(bf16[2560,1536]{1,0:T(8,128)(2,1)} %get-tuple-element.27, bf16[2560,512]{1,0:T(8,128)(2,1)} %all-gather.7.cloned.1.call-done), kind=kOutput, calls=%fused_computation.27 | convolution fusion | flops 4028104704 | bytes 12058624 | tf_op jit(solution)/shard_map/dot_general | solution.py:10
  333.4 0.0 all-reduce.7.cloned.1.call-update
  333.4 0.2 all-gather.9.cloned.1.call-start
  333.6 9.5 %fusion.20 = bf16[512,1536]{0,1:T(8,128)(2,1)} fusion(bf16[2560,1536]{1,0:T(8,128)(2,1)} %get-tuple-element.28, bf16[2560,512]{1,0:T(8,128)(2,1)} %all-gather.7.cloned.1.call-done), kind=kOutput, calls=%fused_computation.28 | convolution fusion | flops 4028104704 | bytes 12058624 | tf_op jit(solution)/shard_map/dot_general | solution.py:10
  343.2 0.0 all-gather.9.cloned.1.call-update
  343.2 0.0 reduce-scatter.2.cloned.1.call-start
  343.3 6.8 %fusion.22 = f32[2560,512]{1,0:T(8,128)S(1)} fusion(bf16[2560,1536]{1,0:T(8,128)(2,1)} %get-tuple-element.28, bf16[512,1536]{1,0:T(8,128)(2,1)S(1)} %copy-done.4), kind=kOutput, calls=%fused_computation.30 | convolution fusion | flops 4026531840 | bytes 14680064 | tf_op jit(solution)/shard_map/dot_general | solution.py:16
  350.1 9.2 %add_convert_fusion = bf16[2560,512]{1,0:T(8,128)(2,1)} fusion(f32[2560,512]{1,0:T(8,128)S(1)} %fusion.22, bf16[2560,1536]{1,0:T(8,128)(2,1)} %get-tuple-element.27, bf16[512,1536]{1,0:T(8,128)(2,1)S(1)} %copy-done.5), kind=kOutput, calls=%fused_computation.17 | convolution fusion | flops 4029153280 | bytes 17301504 | tf_op jit(solution)/shard_map/dot_general | solution.py:16
  359.3 0.0 reduce-scatter.2.cloned.1.call-update
  359.4 60.0 %all-reduce.7.cloned.1.call-done = (bf16[512,1536]{0,1:T(8,128)(2,1)}, bf16[1536,512]{1,0:T(8,128)(2,1)}) async-done(((bf16[512,1536]{0,1:T(8,128)(2,1)}, bf16[1536,512]{1,0:T(8,128)(2,1)}), (bf16[512,1536]{0,1:T(8,128)(2,1)}, bf16[1536,512]{1,0:T(8,128)(2,1)})) %all-reduce.7.cloned.1.call-update) | async-done | bytes 3145744 | tf_op jit(solution)/shard_map/psum | solution.py:66
  419.4 3.2 copy.16
  422.6 2.0 multiply_reduce_fusion
  424.6 12.5 %psum.47 = f32[1536]{0:T(1024)} all-reduce(f32[1536]{0:T(1024)S(1)} %get-tuple-element.25), channel_id=1, replica_groups=mesh['rep'=4,'fs'=2,'tp'=4] {'tp'}, use_global_device_ids=true, to_apply=%region_10.0 | all-reduce | flops 1536 | bytes 12288 | tf_op jit(solution)/shard_map/psum | solution.py:26
  437.0 0.4 multiply_reduce_fusion.1
  437.4 54.1 %all-gather.9.cloned.1.call-done = bf16[2048,1536]{0,1:T(8,128)(2,1)} async-done(((bf16[512,1536]{0,1:T(8,128)(2,1)}), bf16[2048,1536]{0,1:T(8,128)(2,1)}) %all-gather.9.cloned.1.call-update) | async-done | bytes 6291472 | tf_op jit(solution)/shard_map/all_gather | solution.py:61
  491.5 11.3 %reshape.14 = bf16[4,512,1536]{1,0,2:T(4,128)(2,1)} reshape(bf16[2048,1536]{0,1:T(8,128)(2,1)} %all-gather.9.cloned.1.call-done) | data formatting | bytes 12582912 | tf_op jit(solution)/shard_map/all_gather | solution.py:61
  502.9 10.6 %reduce_sum.39 = bf16[512,1536]{0,1:T(8,128)(2,1)S(1)} reduce(bf16[4,512,1536]{1,0,2:T(4,128)(2,1)} %reshape.14, bf16[]{:T(256)} %constant.3.clone.1), dimensions={0}, to_apply=%region_2.0 | reduce | flops 2359296 | bytes 7864322 | tf_op jit(solution)/shard_map/reduce_sum | solution.py:61
  513.5 2.1 copy.15
  515.5 0.4 multiply_reduce_fusion.2
  515.9 3.0 all-reduce
  (14 shorter events, 0.0 us)
Async XLA Ops:
  7.2 16.5 %copy-start = (bf16[1536,512]{1,0:T(8,128)(2,1)S(1)}, bf16[1536,512]{1,0:T(8,128)(2,1)}, u32[]{:S(2)}) copy-start(bf16[1536,512]{1,0:T(8,128)(2,1)} %param.13) | copy-start | bytes 4718596
  7.2 16.5 %all-gather.5.cloned.1.call-start = ((), (), s32[]{:S(2)}) async-start(), calls=%async_computation.1 | async-start | bytes 3932160 | tf_op jit(solution)/shard_map/all_gather | solution.py:33
  7.9 299.0 %all-reduce.5.cloned.1.call-start = ((), (), s32[]{:S(2)}) async-start(), calls=%async_computation.2 | async-start | bytes 15728640 | tf_op jit(solution)/shard_map/psum | solution.py:35
  31.8 292.2 %all-gather.7.cloned.1.call-start = ((), (), s32[]{:S(2)}) async-start(), calls=%async_computation.4 | async-start | bytes 3932160 | tf_op jit(solution)/shard_map/all_gather | solution.py:32
  32.5 386.8 %all-reduce.7.cloned.1.call-start = ((), (), s32[]{:S(2)}) async-start(), calls=%async_computation.6 | async-start | bytes 6291456 | tf_op jit(solution)/shard_map/psum | solution.py:66
  333.4 158.2 %all-gather.9.cloned.1.call-start = ((), (), s32[]{:S(2)}) async-start(), calls=%async_computation.5 | async-start | bytes 7864320 | tf_op jit(solution)/shard_map/all_gather | solution.py:61
  333.6 9.6 %copy-start.4 = (bf16[512,1536]{1,0:T(8,128)(2,1)S(1)}, bf16[512,1536]{1,0:T(8,128)(2,1)}, u32[]{:S(2)}) copy-start(bf16[512,1536]{1,0:T(8,128)(2,1)} %param.11) | copy-start | bytes 4718596
  343.2 6.9 %copy-start.5 = (bf16[512,1536]{1,0:T(8,128)(2,1)S(1)}, bf16[512,1536]{1,0:T(8,128)(2,1)}, u32[]{:S(2)}) copy-start(bf16[512,1536]{1,0:T(8,128)(2,1)} %param.12) | copy-start | bytes 4718596
  343.2 175.8 %reduce-scatter.2.cloned.1.call-start = ((), (), s32[]{:S(2)}) async-start(), calls=%async_computation.3 | async-start | bytes 3932160 | tf_op jit(solution)/shard_map/reduce_scatter | solution.py:47
  419.4 3.2 copy-start.3
  419.4 17.7 %copy-start.2 = (bf16[512,1536]{0,1:T(8,128)(2,1)S(1)}, bf16[512,1536]{0,1:T(8,128)(2,1)}, u32[]{:S(2)}) copy-start(bf16[512,1536]{0,1:T(8,128)(2,1)} %get-tuple-element.23) | copy-start | bytes 4718596
  491.5 27.4 %copy-start.1 = (bf16[1536,512]{1,0:T(8,128)(2,1)S(1)}, bf16[1536,512]{1,0:T(8,128)(2,1)}, u32[]{:S(2)}) copy-start(bf16[1536,512]{1,0:T(8,128)(2,1)} %param.13) | copy-start | bytes 4718596
Sparse Core Ops, SparseCore 0:
  9.5 14.0 all-gather.4
  31.9 274.9 all-reduce.4
  308.5 10.1 all-gather.6
  333.5 85.8 all-reduce.6
  421.6 69.8 all-gather.8
  494.2 10.4 reduce-scatter.1
